TPU v7x, 512 devices: a 4x2x32 block of a 4x8x32 slice. The times are simulated.
512 devices in a mesh: grp: 2 (over y), fs: 32 (over z), tp: 8 (over x, core).
Axes of the slice: x: 4, y: 2, z: 32, core: 2. Of those that a mesh axis runs over, the one named last changes fastest.
The devices are a block of a 4x8x32 slice.
Arguments:
- tokens: bfloat16 [20480, 2048], P(('grp', 'fs', 'tp')), parts along dimension 0, may hold values from -6 to 6
- mix_gain: bfloat16 [2048], replicated, may hold values from 0.099609375 to 1.8984375
- val_weight: bfloat16 [2048, 1024], P('fs', 'tp'), may hold values from -4 to 4
- gate_weight: bfloat16 [2048, 1024], P('fs', 'tp'), may hold values from -0.125 to 0.125
- conv_taps: bfloat16 [31, 1024], replicated, may hold values from -1 to 1
- chan_gain: bfloat16 [1024], replicated, may hold values from 0.099609375 to 1.8984375
- out_weight: bfloat16 [1024, 2048], P('tp', 'fs'), may hold values from -0.1875 to 0.1875
- mix_post_gain: bfloat16 [2048], replicated, may hold values from 0.099609375 to 1.8984375
- ffn_gain: bfloat16 [2048], replicated, may hold values from 0.099609375 to 1.8984375
- up_gate_weight: bfloat16 [2048, 5120], P('fs', 'tp'), may hold values from -0.125 to 0.125
- up_val_weight: bfloat16 [2048, 5120], P('fs', 'tp'), may hold values from -0.125 to 0.125
- ffn_taps: bfloat16 [2, 3, 5120], replicated, may hold values from -3.5 to 3.5
- down_weight: bfloat16 [5120, 2048], P('tp', 'fs'), may hold values from -0.078125 to 0.078125
- ffn_post_gain: bfloat16 [2048], replicated, may hold values from 0.099609375 to 1.8984375
Outputs:
- layer_out: bfloat16 [20480, 2048], P(('grp', 'fs', 'tp')), parts along dimension 0
There are 2 independent parts, one for each index of `grp`. A program takes and returns all parts, laid end to end along the dimension named above; an argument that names none is the same for every part. Nothing has to cross between parts.
All inputs are finite; a program needn't handle non-finite values.
Results may differ from a plain program's by a relative error of at most 0.019.
Values may be sent and summed in bfloat16 or wider, within the bound.
A program may use at most 64 MiB of HBM per device.

v0:
```python
import jax
import jax.numpy as jnp
from jax import lax
from jax.sharding import PartitionSpec as P

LEN = 64
norm_epsilon = 1e-06
chan_epsilon = 1e-05


def from_everyone(array, axis):
    copies = jnp.broadcast_to(array, (lax.axis_size(axis), *array.shape))
    return lax.all_to_all(copies, axis, split_axis=0, concat_axis=0, tiled=True)


def laid_out(blocks, dim):
    blocks = jnp.moveaxis(blocks, 0, dim)
    lengths = blocks.shape
    return blocks.reshape(*lengths[:dim], lengths[dim] * lengths[dim + 1], *lengths[dim + 2 :])


def gathered_copies(array, axis, dim):
    blocks = from_everyone(array, axis)
    return laid_out(blocks, dim)


def sent_together(arrays, axis, dim, along):
    ends, at = ([], 0)
    for a in arrays[:-1]:
        at += a.shape[along]
        ends.append(at)
    both = jnp.concatenate(arrays, axis=along)
    return tuple(jnp.split(lax.all_gather(both, axis, axis=dim, tiled=True), ends, axis=along))


def over_copies(array, axis):
    return from_everyone(array, axis).sum(axis=0)


def together(arrays, axis):
    ends = [0]
    for a in arrays:
        ends.append(ends[-1] + a.size)
    total = over_copies(jnp.concatenate([a.ravel() for a in arrays]), axis)
    return tuple((total[b:e].reshape(a.shape) for a, b, e in zip(arrays, ends, ends[1:])))


def in_blocks(array, dim, length):
    lengths = array.shape
    blocks = array.reshape(*lengths[:dim], length, lengths[dim] // length, *lengths[dim + 1 :])
    return jnp.moveaxis(blocks, dim, 0)


def summed_on_arrival(array, axis, dim):
    blocks = in_blocks(array, dim, lax.axis_size(axis))
    arrived = lax.all_to_all(blocks, axis, split_axis=0, concat_axis=0, tiled=True)
    return arrived.astype(jnp.float32).sum(axis=0)


def rms_scale(values, gain):
    inverse = lax.rsqrt(jnp.mean(values * values, axis=-1, keepdims=True) + norm_epsilon)
    return values * inverse * gain.astype(jnp.float32)


def depthwise(signal, tap_table):
    taps_count = tap_table.shape[0]
    channels = signal.shape[1]
    shaped = signal.astype(jnp.float32).reshape(signal.shape[0] // LEN, LEN, channels)
    padded = jnp.pad(shaped, ((0, 0), (taps_count - 1, 0), (0, 0)))
    tap_values = tap_table.astype(jnp.float32)
    result = jnp.zeros(shaped.shape, jnp.float32)
    for offset in range(taps_count):
        result = result + padded[:, offset : offset + LEN, :] * tap_values[offset]
    return result.reshape(signal.shape[0], channels)


def make_adder(left, pieces):
    first = jnp.dot(left, pieces[0], preferred_element_type=jnp.float32)
    second = jnp.dot(left, pieces[1], preferred_element_type=jnp.float32)
    return (first, second)


def make_rows_product(left, weight):
    return jnp.dot(left, weight, preferred_element_type=jnp.float32)


def shards(
    tokens,
    mix_gain,
    val_weight,
    gate_weight,
    conv_taps,
    chan_gain,
    out_weight,
    mix_post_gain,
    ffn_gain,
    up_gate_weight,
    up_val_weight,
    ffn_taps,
    down_weight,
    ffn_post_gain,
):
    member = lax.axis_index("tp")
    normed_own = rms_scale(tokens.astype(jnp.float32), mix_gain).astype(jnp.bfloat16)
    normed = gathered_copies(normed_own, "tp", 0)
    local_ch = val_weight.shape[1]
    values, gate_sums = make_adder(normed, sent_together((val_weight, gate_weight), "fs", 0, 1))
    glu_out = (values * jax.nn.sigmoid(gate_sums)).astype(jnp.bfloat16)
    own_taps = lax.dynamic_slice_in_dim(conv_taps, member * local_ch, local_ch, 1)
    conv_out = depthwise(glu_out, own_taps)
    totals, squares = together(
        (jnp.sum(conv_out, axis=1), jnp.sum(conv_out * conv_out, axis=1)), "tp"
    )
    all_channels = chan_gain.shape[0]
    chan_mean = totals[:, None] / all_channels
    chan_var = squares[:, None] / all_channels - chan_mean * chan_mean
    own_gain = lax.dynamic_slice_in_dim(chan_gain, member * local_ch, local_ch, 0).astype(
        jnp.float32
    )
    activated = jax.nn.silu((conv_out - chan_mean) * lax.rsqrt(chan_var + chan_epsilon) * own_gain)
    activated = activated.astype(jnp.bfloat16)
    out_full = lax.all_gather(out_weight, "fs", axis=1, tiled=True)
    mixed_sum = summed_on_arrival(
        make_rows_product(activated, out_full).astype(jnp.bfloat16), "tp", 0
    )
    residual = (tokens.astype(jnp.float32) + rms_scale(mixed_sum, mix_post_gain)).astype(
        jnp.bfloat16
    )
    normed_share = rms_scale(residual.astype(jnp.float32), ffn_gain).astype(jnp.bfloat16)
    normed_ffn = gathered_copies(normed_share, "tp", 0)
    local_ff = up_gate_weight.shape[1]
    own_ffn_taps = lax.dynamic_slice_in_dim(ffn_taps, member * local_ff, local_ff, 2)
    gate_full, val_full = sent_together((up_gate_weight, up_val_weight), "fs", 0, 1)
    up_gate = jnp.dot(normed_ffn, gate_full, preferred_element_type=jnp.float32).astype(
        jnp.bfloat16
    )
    up_val = jnp.dot(normed_ffn, val_full, preferred_element_type=jnp.float32).astype(jnp.bfloat16)
    gate_conv = depthwise(up_gate, own_ffn_taps[0])
    val_conv = depthwise(up_val, own_ffn_taps[1])
    hidden = (jax.nn.gelu(gate_conv, approximate=True) * val_conv).astype(jnp.bfloat16)
    down_full = lax.all_gather(down_weight, "fs", axis=1, tiled=True)
    ffn_sum = summed_on_arrival(make_rows_product(hidden, down_full).astype(jnp.bfloat16), "tp", 0)
    return (residual.astype(jnp.float32) + rms_scale(ffn_sum, ffn_post_gain)).astype(jnp.bfloat16)


def solution(mesh):
    return jax.shard_map(
        shards,
        mesh=mesh,
        in_specs=(
            P(("grp", "fs", "tp"), None),
            P(),
            P("fs", "tp"),
            P("fs", "tp"),
            P(),
            P(),
            P("tp", "fs"),
            P(),
            P(),
            P("fs", "tp"),
            P("fs", "tp"),
            P(),
            P("tp", "fs"),
            P(),
        ),
        out_specs=P(("grp", "fs", "tp"), None),
        check_vma=False,
    )
```

profile of v0, /device:TPU:33, one launch (start us, length us, event | category | flops | bytes accessed | tf_op | source)
XLA Modules:
  0.0 472.4 jit_solution(905065115232511449)
XLA Ops:
  6.6 1.3 pad_maximum_fusion.1
  8.0 1.6 pad_maximum_fusion
  10.4 1.1 fusion.33
  11.5 1.0 fusion.35
  12.5 1.3 broadcast_in_dim.6
  13.7 45.0 %all-to-all-start = ((bf16[8,40,2048]{2,1,0:T(8,128)(2,1)}), bf16[8,40,2048]{2,1,0:T(8,128)(2,1)S(1)}, u32[]{:S(2)}, u32[]{:S(2)}) async-start(bf16[8,40,2048]{2,1,0:T(8,128)(2,1)} %broadcast_in_dim.6), calls=%async_computation | async-start | bytes 2621440 | tf_op jit(solution)/shard_map/all_to_all | solution.py:13
  59.5 46.8 %all_gather.13 = bf16[128,2048]{0,1:T(8,128)(2,1)S(1)} all-gather(bf16[128,64]{0,1:T(8,128)(2,1)S(1)} %copy-done.2), channel_id=1, replica_groups=mesh['grp'=2,'fs'=32,'tp'=8] {'fs'}, dimensions={1}, use_global_device_ids=true | all-gather | bytes 540672 | tf_op jit(solution)/shard_map/all_gather | solution.py:122
  106.3 43.0 %all-gather.4.cloned.1.call-done = bf16[2048,256]{1,0:T(8,128)(2,1)} async-done(((bf16[64,256]{1,0:T(8,128)(2,1)}), bf16[2048,256]{1,0:T(8,128)(2,1)}) %all-gather.4.cloned.1.call-update) | async-done | bytes 1048592 | tf_op jit(solution)/shard_map/all_gather | solution.py:33
  149.3 1.6 fusion.12
  153.0 25.4 %all-to-all-start.1 = ((f32[8,1,640]{2,1,0:T(1,128)}), f32[8,1,640]{2,1,0:T(1,128)S(1)}, u32[]{:S(2)}, u32[]{:S(2)}) async-start(f32[8,1,640]{2,1,0:T(1,128)} %broadcast_in_dim.7), calls=%async_computation.1 | async-start | bytes 40960 | tf_op jit(solution)/shard_map/all_to_all | solution.py:13
  179.2 3.9 all-to-all-done.1
  183.4 1.7 convolution_convert_fusion
  185.1 4.3 all-to-all-start.2
  190.2 17.1 %all-to-all-done.2 = bf16[8,40,2048]{2,1,0:T(8,128)(2,1)S(1)} async-done(((bf16[8,40,2048]{2,1,0:T(8,128)(2,1)}), bf16[8,40,2048]{2,1,0:T(8,128)(2,1)S(1)}, u32[]{:S(2)}, u32[]{:S(2)}) %all-to-all-start.2) | async-done | bytes 1310752 | tf_op jit(solution)/shard_map/all_to_all | solution.py:56
  208.0 1.3 broadcast_in_dim.8
  209.3 4.4 all-to-all-start.3
  214.7 17.0 %all-to-all-done.3 = bf16[8,40,2048]{2,1,0:T(8,128)(2,1)S(1)} async-done(((bf16[8,40,2048]{2,1,0:T(8,128)(2,1)}), bf16[8,40,2048]{2,1,0:T(8,128)(2,1)S(1)}, u32[]{:S(2)}, u32[]{:S(2)}) %all-to-all-start.3) | async-done | bytes 1310752 | tf_op jit(solution)/shard_map/all_to_all | solution.py:13
  231.6 55.6 %all-gather.6.cloned.1.call-done = bf16[2048,1280]{1,0:T(8,128)(2,1)} async-done(((bf16[64,1280]{1,0:T(8,128)(2,1)}), bf16[2048,1280]{1,0:T(8,128)(2,1)}) %all-gather.6.cloned.1.call-update) | async-done | bytes 5242896 | tf_op jit(solution)/shard_map/all_gather | solution.py:33
  287.2 3.1 fusion.4
  290.5 1.2 fusion.7
  292.5 124.9 %all-gather.8.cloned.1.call-done = bf16[640,2048]{0,1:T(8,128)(2,1)} async-done(((bf16[640,64]{0,1:T(8,128)(2,1)}), bf16[640,2048]{0,1:T(8,128)(2,1)}) %all-gather.8.cloned.1.call-update) | async-done | bytes 2621456 | tf_op jit(solution)/shard_map/all_gather | solution.py:141
  417.5 4.0 convolution_convert_fusion.1
  421.5 25.5 %all-to-all-start.4 = ((bf16[8,40,2048]{2,1,0:T(8,128)(2,1)}), bf16[8,40,2048]{2,1,0:T(8,128)(2,1)S(1)}, u32[]{:S(2)}, u32[]{:S(2)}) async-start(bf16[8,40,2048]{2,1,0:T(8,128)(2,1)} %bitcast.43), calls=%async_computation.4 | async-start | bytes 2621440 | tf_op jit(solution)/shard_map/all_to_all | solution.py:56
  447.0 17.8 %all-to-all-done.4 = bf16[8,40,2048]{2,1,0:T(8,128)(2,1)S(1)} async-done(((bf16[8,40,2048]{2,1,0:T(8,128)(2,1)}), bf16[8,40,2048]{2,1,0:T(8,128)(2,1)S(1)}, u32[]{:S(2)}, u32[]{:S(2)}) %all-to-all-start.4) | async-done | bytes 1310752 | tf_op jit(solution)/shard_map/all_to_all | solution.py:56
  (57 shorter events, 9.1 us)
Async XLA Ops:
  6.5 142.8 %all-gather.4.cloned.1.call-start = ((), (), s32[]{:S(2)}) async-start(), calls=%async_computation.5 | async-start | bytes 1081344 | tf_op jit(solution)/shard_map/all_gather | solution.py:33
  8.0 279.3 %all-gather.6.cloned.1.call-start = ((), (), s32[]{:S(2)}) async-start(), calls=%async_computation.6 | async-start | bytes 5406720 | tf_op jit(solution)/shard_map/all_gather | solution.py:33
  13.7 45.8 %copy-start.2 = (bf16[128,64]{0,1:T(8,128)(2,1)S(1)}, bf16[128,64]{0,1:T(8,128)(2,1)}, u32[]{:S(2)}) copy-start(bf16[128,64]{0,1:T(8,128)(2,1)} %param.20) | copy-start | bytes 49156
  13.7 92.6 %all-to-all-start = ((bf16[8,40,2048]{2,1,0:T(8,128)(2,1)}), bf16[8,40,2048]{2,1,0:T(8,128)(2,1)S(1)}, u32[]{:S(2)}, u32[]{:S(2)}) async-start(bf16[8,40,2048]{2,1,0:T(8,128)(2,1)} %broadcast_in_dim.6), calls=%async_computation | async-start | bytes 2621440 | tf_op jit(solution)/shard_map/all_to_all | solution.py:13
  149.3 1.7 copy-start.1
  153.0 30.1 %all-to-all-start.1 = ((f32[8,1,640]{2,1,0:T(1,128)}), f32[8,1,640]{2,1,0:T(1,128)S(1)}, u32[]{:S(2)}, u32[]{:S(2)}) async-start(f32[8,1,640]{2,1,0:T(1,128)} %broadcast_in_dim.7), calls=%async_computation.1 | async-start | bytes 40960 | tf_op jit(solution)/shard_map/all_to_all | solution.py:13
  185.1 5.1 %copy-start.3 = (bf16[2048]{0:T(1024)(128)(2,1)S(1)}, bf16[2048]{0:T(1024)(128)(2,1)}, u32[]{:S(2)}) copy-start(bf16[2048]{0:T(1024)(128)(2,1)} %param.21) | copy-start | bytes 12292
  185.1 5.1 %copy-start.4 = (bf16[2048]{0:T(1024)(128)(2,1)S(1)}, bf16[2048]{0:T(1024)(128)(2,1)}, u32[]{:S(2)}) copy-start(bf16[2048]{0:T(1024)(128)(2,1)} %param.22) | copy-start | bytes 12292
  185.1 22.2 %all-to-all-start.2 = ((bf16[8,40,2048]{2,1,0:T(8,128)(2,1)}), bf16[8,40,2048]{2,1,0:T(8,128)(2,1)S(1)}, u32[]{:S(2)}, u32[]{:S(2)}) async-start(bf16[8,40,2048]{2,1,0:T(8,128)(2,1)} %bitcast.35), calls=%async_computation.2 | async-start | bytes 2621440 | tf_op jit(solution)/shard_map/all_to_all | solution.py:56
  189.4 18.2 %copy-start = (bf16[40,2048]{1,0:T(8,128)(2,1)S(1)}, bf16[40,2048]{1,0:T(8,128)(2,1)}, u32[]{:S(2)}) copy-start(bf16[40,2048]{1,0:T(8,128)(2,1)} %param.14) | copy-start | bytes 491524
  189.4 228.1 %all-gather.8.cloned.1.call-start = ((), (), s32[]{:S(2)}) async-start(), calls=%async_computation.7 | async-start | bytes 2703360 | tf_op jit(solution)/shard_map/all_gather | solution.py:141
  209.3 22.3 %all-to-all-start.3 = ((bf16[8,40,2048]{2,1,0:T(8,128)(2,1)}), bf16[8,40,2048]{2,1,0:T(8,128)(2,1)S(1)}, u32[]{:S(2)}, u32[]{:S(2)}) async-start(bf16[8,40,2048]{2,1,0:T(8,128)(2,1)} %broadcast_in_dim.8), calls=%async_computation.3 | async-start | bytes 2621440 | tf_op jit(solution)/shard_map/all_to_all | solution.py:13
  287.2 3.3 copy-start.6
  421.5 25.5 %copy-start.5 = (bf16[2048]{0:T(1024)(128)(2,1)S(1)}, bf16[2048]{0:T(1024)(128)(2,1)}, u32[]{:S(2)}) copy-start(bf16[2048]{0:T(1024)(128)(2,1)} %param.27) | copy-start | bytes 12292
  421.5 43.3 %all-to-all-start.4 = ((bf16[8,40,2048]{2,1,0:T(8,128)(2,1)}), bf16[8,40,2048]{2,1,0:T(8,128)(2,1)S(1)}, u32[]{:S(2)}, u32[]{:S(2)}) async-start(bf16[8,40,2048]{2,1,0:T(8,128)(2,1)} %bitcast.43), calls=%async_computation.4 | async-start | bytes 2621440 | tf_op jit(solution)/shard_map/all_to_all | solution.py:56
Sparse Core Ops, SparseCore 0:
  9.4 139.8 all-gather.3
  151.4 135.7 all-gather.5
  289.3 128.1 all-gather.7
where the time goes:
time: 473 us; the launch traced here: 472 us
  waiting for transfers between devices  280 us (59%)
  starting transfers between devices  105 us (22%)
  blocking collectives  46.8 us (10%)
  between operations  13.3 us (3%)
  matrix products  12.1 us (3%)
  other arithmetic  11.8 us (2%)
    all_gather x1, waiting for transfers between devices, shards(): down_full = lax.all_gather(down_weight, 'fs', axis=1, tiled=True)  125 us
    all_gather x2, waiting for transfers between devices, sent_together(): lax.all_gather(both, axis, axis=dim, tiled=True)  98.6 us
    all_to_all x3, starting transfers between devices, from_everyone(): return lax.all_to_all(copies, axis, split_axis=0, concat_axis=0, tiled=True)  74.9 us
    all_gather x1, blocking collectives, shards(): out_full = lax.all_gather(out_weight, 'fs', axis=1, tiled=True)  46.8 us
    all_to_all x2, waiting for transfers between devices, summed_on_arrival(): lax.all_to_all(blocks, axis, split_axis=0, concat_axis=0, tiled=True)  34.8 us
    all_to_all x2, starting transfers between devices, summed_on_arrival(): lax.all_to_all(blocks, axis, split_axis=0, concat_axis=0, tiled=True)  29.8 us
    all_to_all x3, waiting for transfers between devices, from_everyone(): return lax.all_to_all(copies, axis, split_axis=0, concat_axis=0, tiled=True)  20.9 us
  transfers between devices with their start and end apart: 8, of which 7 were waited for; matrix products, arithmetic and copies ran while one was open for 4% of the time, Pallas kernels for 0%

commit v1 on v0

--- a/solution.py
+++ b/solution.py
@@ -138,7 +138,9 @@
     gate_conv = depthwise(up_gate, own_ffn_taps[0])
     val_conv = depthwise(up_val, own_ffn_taps[1])
     hidden = (jax.nn.gelu(gate_conv, approximate=True) * val_conv).astype(jnp.bfloat16)
-    down_full = lax.all_gather(down_weight, "fs", axis=1, tiled=True)
+    down_full = jnp.concatenate(
+        lax.all_to_all(jnp.stack([down_weight] * lax.axis_size("fs")), "fs", 0, 0), axis=1
+    )
     ffn_sum = summed_on_arrival(make_rows_product(hidden, down_full).astype(jnp.bfloat16), "tp", 0)
     return (residual.astype(jnp.float32) + rms_scale(ffn_sum, ffn_post_gain)).astype(jnp.bfloat16)
 

time: 473 us -> 603 us (1.27)
  waiting for transfers between devices: 280 us -> 389 us
  blocking collectives: 46.8 us -> 69.8 us
    all_gather x2, waiting for transfers between devices: 98.6 us -> 349 us  [sent_together(): lax.all_gather(both, axis, axis=dim, tiled=True)]
    all_gather x1 -> x0, waiting for transfers between devices: 125 us -> none  [shards(): down_full = lax.all_gather(down_weight, 'fs', axis=1, tiled=True)]
    all_to_all x0 -> x1, blocking collectives: none -> 22 us  [from_everyone(): return lax.all_to_all(copies, axis, split_axis=0, concat_axis=0, tiled=True)]
    all_to_all x3 -> x2, waiting for transfers between devices: 20.9 us -> 3.92 us  [from_everyone(): return lax.all_to_all(copies, axis, split_axis=0, concat_axis=0, tiled=True)]
    all_to_all x0 -> x1, starting transfers between devices: none -> 13 us  [shards(): lax.all_to_all(jnp.stack([down_weight] * lax.axis_size('fs')), 'fs', 0, 0)]
    all_to_all x2, starting transfers between devices: 29.8 us -> 19.6 us  [summed_on_arrival(): lax.all_to_all(blocks, axis, split_axis=0, concat_axis=0, tiled=True)]
    all_to_all x3 -> x2, starting transfers between devices: 74.9 us -> 71.1 us  [from_everyone(): return lax.all_to_all(copies, axis, split_axis=0, concat_axis=0, tiled=True)]
  transfers between devices with their start and end apart: 8 -> 7, of which waited for: 7 -> 5; matrix products, arithmetic and copies ran while one was open for 4% -> 2% of each run, Pallas kernels for 0% -> 0%
where the time goes in v1:
time: 603 us; the launch traced here: 602 us
  waiting for transfers between devices  389 us (65%)
  starting transfers between devices  104 us (17%)
  blocking collectives  69.8 us (12%)
  between operations  13.7 us (2%)
  other arithmetic  10.9 us (2%)
  matrix products  10.7 us (2%)
    all_gather x2, waiting for transfers between devices, sent_together(): lax.all_gather(both, axis, axis=dim, tiled=True)  349 us
    all_to_all x2, starting transfers between devices, from_everyone(): return lax.all_to_all(copies, axis, split_axis=0, concat_axis=0, tiled=True)  71.1 us
    all_gather x1, blocking collectives, shards(): out_full = lax.all_gather(out_weight, 'fs', axis=1, tiled=True)  47.8 us
    all_to_all x2, waiting for transfers between devices, summed_on_arrival(): lax.all_to_all(blocks, axis, split_axis=0, concat_axis=0, tiled=True)  35.7 us
    all_to_all x1, blocking collectives, from_everyone(): return lax.all_to_all(copies, axis, split_axis=0, concat_axis=0, tiled=True)  22 us
    all_to_all x2, starting transfers between devices, summed_on_arrival(): lax.all_to_all(blocks, axis, split_axis=0, concat_axis=0, tiled=True)  19.6 us
    all_to_all x1, starting transfers between devices, shards(): lax.all_to_all(jnp.stack([down_weight] * lax.axis_size('fs')), 'fs', 0, 0)  13 us
  transfers between devices with their start and end apart: 7, of which 5 were waited for; matrix products, arithmetic and copies ran while one was open for 2% of the time, Pallas kernels for 0%

profile of v1, /device:TPU:33, one launch (start us, length us, event | category | flops | bytes accessed | tf_op | source)
XLA Modules:
  0.0 602.3 jit_solution(16608837954158282103)
XLA Ops:
  6.6 1.4 pad_maximum_fusion.1
  8.7 1.1 fusion.33
  9.7 1.0 fusion.35
  10.8 1.2 broadcast_in_dim.6
  12.0 45.0 %all-to-all-start = ((bf16[8,40,2048]{2,1,0:T(8,128)(2,1)}), bf16[8,40,2048]{2,1,0:T(8,128)(2,1)S(1)}, u32[]{:S(2)}, u32[]{:S(2)}) async-start(bf16[8,40,2048]{2,1,0:T(8,128)(2,1)} %broadcast_in_dim.6), calls=%async_computation | async-start | bytes 2621440 | tf_op jit(solution)/shard_map/all_to_all | solution.py:13
  57.8 47.8 %all_gather.10 = bf16[128,2048]{0,1:T(8,128)(2,1)S(1)} all-gather(bf16[128,64]{0,1:T(8,128)(2,1)S(1)} %copy-done.6), channel_id=1, replica_groups=mesh['grp'=2,'fs'=32,'tp'=8] {'fs'}, dimensions={1}, use_global_device_ids=true | all-gather | bytes 540672 | tf_op jit(solution)/shard_map/all_gather | solution.py:122
  105.5 43.3 %all-gather.3.cloned.1.call-done = bf16[2048,256]{1,0:T(8,128)(2,1)} async-done(((bf16[64,256]{1,0:T(8,128)(2,1)}), bf16[2048,256]{1,0:T(8,128)(2,1)}) %all-gather.3.cloned.1.call-update) | async-done | bytes 1048592 | tf_op jit(solution)/shard_map/all_gather | solution.py:33
  148.8 1.6 fusion.12
  152.5 26.1 %all-to-all-start.1 = ((f32[8,1,640]{2,1,0:T(1,128)}), f32[8,1,640]{2,1,0:T(1,128)S(1)}, u32[]{:S(2)}, u32[]{:S(2)}) async-start(f32[8,1,640]{2,1,0:T(1,128)} %broadcast_in_dim.7), calls=%async_computation.1 | async-start | bytes 40960 | tf_op jit(solution)/shard_map/all_to_all | solution.py:13
  179.3 3.9 all-to-all-done.1
  183.5 1.6 convolution_convert_fusion
  185.1 4.3 all-to-all-start.2
  189.5 17.8 %all-to-all-done.2 = bf16[8,40,2048]{2,1,0:T(8,128)(2,1)S(1)} async-done(((bf16[8,40,2048]{2,1,0:T(8,128)(2,1)}), bf16[8,40,2048]{2,1,0:T(8,128)(2,1)S(1)}, u32[]{:S(2)}, u32[]{:S(2)}) %all-to-all-start.2) | async-done | bytes 1310752 | tf_op jit(solution)/shard_map/all_to_all | solution.py:56
  208.2 22.0 %all_to_all.31 = bf16[8,40,2048]{2,1,0:T(8,128)(2,1)} all-to-all(bf16[8,40,2048]{2,1,0:T(8,128)(2,1)S(1)} %broadcast_in_dim.8), channel_id=1, replica_groups=mesh['grp'=2,'fs'=32,'tp'=8] {'tp'}, dimensions={0} | all-to-all | bytes 2621440 | tf_op jit(solution)/shard_map/all_to_all | solution.py:13
  230.2 1.9 stack.2
  232.1 13.0 %all-to-all-start.4 = ((bf16[32,640,64]{1,2,0:T(8,128)(2,1)}), bf16[32,640,64]{1,2,0:T(8,128)(2,1)S(1)}, u32[]{:S(2)}, u32[]{:S(2)}) async-start(bf16[32,640,64]{1,2,0:T(8,128)(2,1)} %stack.2), calls=%async_computation.4 | async-start | bytes 5242880 | tf_op jit(solution)/shard_map/all_to_all | solution.py:142
  245.9 0.9 dynamic-slice_convert_fusion.2
  246.9 305.9 %all-gather.5.cloned.1.call-done = bf16[2048,1280]{1,0:T(8,128)(2,1)} async-done(((bf16[64,1280]{1,0:T(8,128)(2,1)}), bf16[2048,1280]{1,0:T(8,128)(2,1)}) %all-gather.5.cloned.1.call-update) | async-done | bytes 5242896 | tf_op jit(solution)/shard_map/all_gather | solution.py:33
  552.7 3.5 fusion.4
  556.8 1.2 fusion.7
  558.9 2.3 convolution_convert_fusion.1
  561.2 15.3 %all-to-all-start.5 = ((bf16[8,40,2048]{2,1,0:T(8,128)(2,1)}), bf16[8,40,2048]{2,1,0:T(8,128)(2,1)S(1)}, u32[]{:S(2)}, u32[]{:S(2)}) async-start(bf16[8,40,2048]{2,1,0:T(8,128)(2,1)} %bitcast.97), calls=%async_computation.5 | async-start | bytes 2621440 | tf_op jit(solution)/shard_map/all_to_all | solution.py:56
  576.5 17.9 %all-to-all-done.5 = bf16[8,40,2048]{2,1,0:T(8,128)(2,1)S(1)} async-done(((bf16[8,40,2048]{2,1,0:T(8,128)(2,1)}), bf16[8,40,2048]{2,1,0:T(8,128)(2,1)S(1)}, u32[]{:S(2)}, u32[]{:S(2)}) %all-to-all-start.5) | async-done | bytes 1310752 | tf_op jit(solution)/shard_map/all_to_all | solution.py:56
  594.7 0.8 fusion.40
  (62 shorter events, 8.0 us)
Async XLA Ops:
  6.5 142.3 %all-gather.3.cloned.1.call-start = ((), (), s32[]{:S(2)}) async-start(), calls=%async_computation.6 | async-start | bytes 1081344 | tf_op jit(solution)/shard_map/all_gather | solution.py:33
  12.0 45.8 %copy-start.6 = (bf16[128,64]{0,1:T(8,128)(2,1)S(1)}, bf16[128,64]{0,1:T(8,128)(2,1)}, u32[]{:S(2)}) copy-start(bf16[128,64]{0,1:T(8,128)(2,1)} %param.20) | copy-start | bytes 49156
  12.0 93.5 %all-to-all-start = ((bf16[8,40,2048]{2,1,0:T(8,128)(2,1)}), bf16[8,40,2048]{2,1,0:T(8,128)(2,1)S(1)}, u32[]{:S(2)}, u32[]{:S(2)}) async-start(bf16[8,40,2048]{2,1,0:T(8,128)(2,1)} %broadcast_in_dim.6), calls=%async_computation | async-start | bytes 2621440 | tf_op jit(solution)/shard_map/all_to_all | solution.py:13
  148.8 1.7 copy-start.2
  152.5 30.7 %all-to-all-start.1 = ((f32[8,1,640]{2,1,0:T(1,128)}), f32[8,1,640]{2,1,0:T(1,128)S(1)}, u32[]{:S(2)}, u32[]{:S(2)}) async-start(f32[8,1,640]{2,1,0:T(1,128)} %broadcast_in_dim.7), calls=%async_computation.1 | async-start | bytes 40960 | tf_op jit(solution)/shard_map/all_to_all | solution.py:13
  185.1 4.3 copy-start.7
  185.1 4.3 copy-start.8
  185.1 22.2 %all-to-all-start.2 = ((bf16[8,40,2048]{2,1,0:T(8,128)(2,1)}), bf16[8,40,2048]{2,1,0:T(8,128)(2,1)S(1)}, u32[]{:S(2)}, u32[]{:S(2)}) async-start(bf16[8,40,2048]{2,1,0:T(8,128)(2,1)} %bitcast.35), calls=%async_computation.2 | async-start | bytes 2621440 | tf_op jit(solution)/shard_map/all_to_all | solution.py:56
  189.4 18.2 %copy-start = (bf16[40,2048]{1,0:T(8,128)(2,1)S(1)}, bf16[40,2048]{1,0:T(8,128)(2,1)}, u32[]{:S(2)}) copy-start(bf16[40,2048]{1,0:T(8,128)(2,1)} %param.14) | copy-start | bytes 491524
  208.2 22.0 %copy-start.5 = (bf16[640,64]{0,1:T(8,128)(2,1)S(1)}, bf16[640,64]{0,1:T(8,128)(2,1)}, u32[]{:S(2)}) copy-start(bf16[640,64]{0,1:T(8,128)(2,1)} %param.26) | copy-start | bytes 245764
  232.1 13.1 %copy-start.3 = (bf16[64,640]{1,0:T(8,128)(2,1)S(1)}, bf16[64,640]{1,0:T(8,128)(2,1)}, u32[]{:S(2)}) copy-start(bf16[64,640]{1,0:T(8,128)(2,1)} %param.24) | copy-start | bytes 245764
  232.1 13.1 %copy-start.4 = (bf16[64,640]{1,0:T(8,128)(2,1)S(1)}, bf16[64,640]{1,0:T(8,128)(2,1)}, u32[]{:S(2)}) copy-start(bf16[64,640]{1,0:T(8,128)(2,1)} %param.23) | copy-start | bytes 245764
  232.1 326.8 %all-to-all-start.4 = ((bf16[32,640,64]{1,2,0:T(8,128)(2,1)}), bf16[32,640,64]{1,2,0:T(8,128)(2,1)S(1)}, u32[]{:S(2)}, u32[]{:S(2)}) async-start(bf16[32,640,64]{1,2,0:T(8,128)(2,1)} %stack.2), calls=%async_computation.4 | async-start | bytes 5242880 | tf_op jit(solution)/shard_map/all_to_all | solution.py:142
  245.1 307.6 %all-gather.5.cloned.1.call-start = ((), (), s32[]{:S(2)}) async-start(), calls=%async_computation.7 | async-start | bytes 5406720 | tf_op jit(solution)/shard_map/all_gather | solution.py:33
  552.7 3.5 copy-start.1
  552.7 4.1 copy-start.10
  561.2 15.3 %copy-start.9 = (bf16[2048]{0:T(1024)(128)(2,1)S(1)}, bf16[2048]{0:T(1024)(128)(2,1)}, u32[]{:S(2)}) copy-start(bf16[2048]{0:T(1024)(128)(2,1)} %param.27) | copy-start | bytes 12292
  561.2 33.2 %all-to-all-start.5 = ((bf16[8,40,2048]{2,1,0:T(8,128)(2,1)}), bf16[8,40,2048]{2,1,0:T(8,128)(2,1)S(1)}, u32[]{:S(2)}, u32[]{:S(2)}) async-start(bf16[8,40,2048]{2,1,0:T(8,128)(2,1)} %bitcast.97), calls=%async_computation.5 | async-start | bytes 2621440 | tf_op jit(solution)/shard_map/all_to_all | solution.py:56
Sparse Core Ops, SparseCore 0:
  9.4 139.3 all-gather.2
  248.0 304.6 all-gather.4
